TPU v7x, 32 devices: a whole 2x2x4 slice. The times are simulated.
32 devices in a mesh: sp: 16 (over z, y, x), tp: 2 (over core).
Axes of the slice: x: 2, y: 2, z: 4, core: 2. Of those that a mesh axis runs over, the one named last changes fastest.
Arguments:
- tokens: bfloat16 [2048, 4096], P('sp'), may hold values from -6 to 6
- norm_gain: float32 [4096], replicated, may hold values from 0.1 to 1.9
- w_query: bfloat16 [4096, 2048], P('sp', 'tp'), may hold values from -1 to 1
- w_key: bfloat16 [4096, 512], P('sp', 'tp'), may hold values from -1 to 1
- w_value: bfloat16 [4096, 512], P('sp', 'tp'), may hold values from -0.09375 to 0.09375
- w_state_in: bfloat16 [4096, 2048], P('sp', 'tp'), may hold values from -0.09375 to 0.09375
- sink_logit: float32 [32], P('tp'), may hold values from 2 to 6
- decay_rate: float32 [128, 64], P('tp'), may hold values from 0.0002 to 4
- rotation: float32 [128, 64], P('tp'), may hold values from 1 to 60
- log_step: float32 [128], P('tp'), may hold values from -5.3 to -3
- in_re: float32 [128, 64, 16], P('tp'), may hold values from -1.5 to 1.5
- in_im: float32 [128, 64, 16], P('tp'), may hold values from -1.5 to 1.5
- out_re: float32 [128, 16, 64], P('tp'), may hold values from -0.75 to 0.75
- out_im: float32 [128, 16, 64], P('tp'), may hold values from -0.75 to 0.75
- skip_gain: float32 [2048], P('tp'), may hold values from -4 to 4
- w_attn_out: bfloat16 [2048, 4096], P('tp', 'sp'), may hold values from -0.5 to 0.5
- w_state_out: bfloat16 [2048, 4096], P('tp', 'sp'), may hold values from -0.125 to 0.125
- out_gain: float32 [4096], replicated, may hold values from 0.1 to 1.9
Outputs:
- mixed: bfloat16 [2048, 4096], P(('sp', 'tp'))
All inputs are finite; a program needn't handle non-finite values.
Results may differ from a plain program's by a relative error of at most 0.015.
The roundings to bfloat16 on the way count: a program that leaves them out, or rounds other values in their place, can miss the bound.
Values may be sent and summed in bfloat16 or wider, within the bound.
No kernel may reach another device: no remote copies, remote signals or barrier semaphores. Data moves between devices by JAX's collectives and lax.ppermute only.
A program may use at most 128 MiB of HBM per device.

v0:
```python
import math
import jax
import jax.numpy as jnp
from jax import lax
from jax.sharding import PartitionSpec as P

HEAD = 64
WINDOW = 128
epsilon = 1e-06
rotary_base = 500000.0


def carried_in(value, axis, join, neutral):
    count, mine = (lax.axis_size(axis), lax.axis_index(axis))
    pieces = jax.tree.map(lambda part: lax.all_gather(part, axis), value)
    so_far = jax.tree.map(
        lambda part, zero: jnp.full_like(part, 0) + jnp.asarray(zero, part.dtype), value, neutral
    )

    def turn(position, so_far):
        longer = join(so_far, jax.tree.map(lambda part: part[position], pieces))
        return jax.tree.map(lambda new, old: jnp.where(position < mine, new, old), longer, so_far)

    return lax.fori_loop(0, count - 1, turn, so_far)


def passed_along(value, axis, by):
    size = lax.axis_size(axis)
    pairs = [(i, i + by) for i in range(size) if 0 <= i + by < size]
    return lax.ppermute(value, axis, pairs)


def rotate(heads_block, positions):
    head_width = heads_block.shape[-1]
    half_width = head_width // 2
    frequency = rotary_base ** (-(jnp.arange(half_width, dtype=jnp.float32) * 2.0 / head_width))
    angles = positions.astype(jnp.float32)[:, None] * frequency[None, :]
    cosine = jnp.cos(angles)[:, None, :]
    sine_part = jnp.sin(angles)[:, None, :]
    lower_half = heads_block[..., :half_width]
    upper_half = heads_block[..., half_width:]
    return jnp.concatenate(
        [
            lower_half * cosine - upper_half * sine_part,
            upper_half * cosine + lower_half * sine_part,
        ],
        axis=-1,
    )


def shape_heads(query_sum, key_sum, value_sum, positions, head_width):
    row_count = query_sum.shape[0]
    kv_heads = key_sum.shape[1] // head_width
    group_size = query_sum.shape[1] // key_sum.shape[1]
    queries = rotate(
        query_sum.reshape(row_count, kv_heads * group_size, head_width), positions
    ).astype(jnp.bfloat16)
    queries = queries.reshape(row_count, kv_heads, group_size, head_width)
    key_rows = rotate(key_sum.reshape(row_count, kv_heads, head_width), positions).astype(
        jnp.bfloat16
    )
    key_rows = key_rows.reshape(row_count, kv_heads * head_width)
    value_rows = value_sum.astype(jnp.bfloat16)
    return (queries, key_rows, value_rows)


def band_attention(queries, key_rows, value_rows, sink_logit, first_row, window):
    row_count, kv_heads, group_size, head_width = queries.shape
    blocks = row_count // window
    query_blocks = queries.reshape(blocks, window, kv_heads, group_size, head_width)
    key_blocks = jnp.concatenate(
        [
            key_rows[:row_count].reshape(blocks, window, kv_heads, head_width),
            key_rows[window:].reshape(blocks, window, kv_heads, head_width),
        ],
        axis=1,
    )
    value_blocks = jnp.concatenate(
        [
            value_rows[:row_count].reshape(blocks, window, kv_heads, head_width),
            value_rows[window:].reshape(blocks, window, kv_heads, head_width),
        ],
        axis=1,
    )
    scores = jnp.einsum(
        "bqkgd,bskd->bkgqs", query_blocks, key_blocks, preferred_element_type=jnp.float32
    ) / math.sqrt(head_width)
    block_start = jnp.arange(blocks, dtype=jnp.int32)[:, None, None] * window
    query_at = first_row + block_start + jnp.arange(window, dtype=jnp.int32)[None, :, None]
    key_at = (
        first_row - window + block_start + jnp.arange(2 * window, dtype=jnp.int32)[None, None, :]
    )
    offset_gap = query_at - key_at
    visible = (offset_gap >= 0) & (offset_gap < window) & (key_at >= 0)
    scores = jnp.where(visible[:, None, None, :, :], scores, -jnp.inf)
    sink_value = sink_logit.reshape(1, kv_heads, group_size, 1, 1)
    top_score = jnp.maximum(jnp.max(scores, axis=-1, keepdims=True), sink_value)
    exponent = jnp.exp(scores - top_score)
    totals = jnp.sum(exponent, axis=-1, keepdims=True) + jnp.exp(sink_value - top_score)
    weights = (exponent / totals).astype(jnp.bfloat16)
    attended = jnp.einsum(
        "bkgqs,bskd->bqkgd", weights, value_blocks, preferred_element_type=jnp.float32
    )
    return attended.reshape(row_count, kv_heads * group_size * head_width).astype(jnp.bfloat16)


def discretize(decay_rate, rotation, log_step, in_re, in_im):
    time_step = jnp.exp(log_step)[:, None]
    lambda_re = -decay_rate
    modulus = jnp.exp(lambda_re * time_step)
    pole_re = modulus * jnp.cos(rotation * time_step)
    pole_im = modulus * jnp.sin(rotation * time_step)
    minus_one = pole_re - 1.0
    denominator = lambda_re * lambda_re + rotation * rotation
    factor_re = ((minus_one * lambda_re + pole_im * rotation) / denominator)[..., None]
    factor_im = ((pole_im * lambda_re - minus_one * rotation) / denominator)[..., None]
    drive_re = factor_re * in_re - factor_im * in_im
    drive_im = factor_re * in_im + factor_im * in_re
    return (pole_re, pole_im, drive_re, drive_im)


def chain_link(earlier, later):
    early_are, early_aim, early_bre, early_bim = earlier
    late_are, late_aim, late_bre, late_bim = later
    return (
        late_are * early_are - late_aim * early_aim,
        late_are * early_aim + late_aim * early_are,
        late_are * early_bre - late_aim * early_bim + late_bre,
        late_are * early_bim + late_aim * early_bre + late_bim,
    )


def local_states(inputs, pole_re, pole_im, drive_re, drive_im):
    row_count = inputs.shape[0]
    groups, states, group_width = drive_re.shape
    channel_values = inputs.astype(jnp.float32).reshape(row_count, groups, group_width)
    push_re = jnp.einsum(
        "tgh,gph->tgp", channel_values, drive_re, precision=lax.Precision.HIGHEST
    ).reshape(row_count, groups * states)
    push_im = jnp.einsum(
        "tgh,gph->tgp", channel_values, drive_im, precision=lax.Precision.HIGHEST
    ).reshape(row_count, groups * states)
    decay_re = jnp.broadcast_to(pole_re.reshape(1, groups * states), push_re.shape)
    decay_im = jnp.broadcast_to(pole_im.reshape(1, groups * states), push_im.shape)
    return lax.associative_scan(chain_link, (decay_re, decay_im, push_re, push_im), axis=0)


def apply_carry(running, carry_re, carry_im):
    power_re, power_im, own_re, own_im = running
    return (
        own_re + power_re * carry_re - power_im * carry_im,
        own_im + power_re * carry_im + power_im * carry_re,
    )


def read_out(inputs, state_re, state_im, out_re, out_im, skip_gain):
    row_count = inputs.shape[0]
    groups, group_width, states = out_re.shape
    grid_re = state_re.reshape(row_count, groups, states)
    grid_im = state_im.reshape(row_count, groups, states)
    summed = jnp.einsum(
        "tgp,ghp->tgh", grid_re, out_re, precision=lax.Precision.HIGHEST
    ) - jnp.einsum("tgp,ghp->tgh", grid_im, out_im, precision=lax.Precision.HIGHEST)
    summed = summed.reshape(row_count, groups * group_width) + skip_gain * inputs.astype(
        jnp.float32
    )
    return jax.nn.gelu(summed).astype(jnp.bfloat16)


def chain_in(power_re, power_im, end_re, end_im):
    identity = (
        jnp.ones_like(power_re),
        jnp.zeros_like(power_im),
        jnp.zeros_like(end_re),
        jnp.zeros_like(end_im),
    )
    before = carried_in((power_re, power_im, end_re, end_im), "sp", chain_link, identity)
    return (before[2], before[3])


def state_branch(inputs, decay_rate, rotation, log_step, in_re, in_im, out_re, out_im, skip_gain):
    pole_re, pole_im, drive_re, drive_im = discretize(decay_rate, rotation, log_step, in_re, in_im)
    running = local_states(inputs, pole_re, pole_im, drive_re, drive_im)
    carry_re, carry_im = chain_in(running[0][-1], running[1][-1], running[2][-1], running[3][-1])
    state_re, state_im = apply_carry(running, carry_re, carry_im)
    return read_out(inputs, state_re, state_im, out_re, out_im, skip_gain)


def earlier_window(key_rows, value_rows):
    joined = jnp.concatenate([key_rows, value_rows], axis=1)
    prior = passed_along(joined, "sp", 1)
    return jnp.concatenate([prior, joined], axis=0)


def make_adder(normed_cols):

    def add_pieces(carried, weight_pieces, row_start):
        updated = []
        for running_total, weight_piece in zip(carried, weight_pieces):
            product = lax.dot_general(
                normed_cols,
                weight_piece,
                (((0,), (0,)), ((), ())),
                preferred_element_type=jnp.float32,
            )
            updated.append(product)
        return tuple(updated)

    return add_pieces


def body(
    tokens,
    norm_gain,
    w_query,
    w_key,
    w_value,
    w_state_in,
    sink_logit,
    decay_rate,
    rotation,
    log_step,
    in_re,
    in_im,
    out_re,
    out_im,
    skip_gain,
    w_attn_out,
    w_state_out,
    out_gain,
):
    row_count = tokens.shape[0]
    window = WINDOW
    head_width = HEAD
    wide_tokens = tokens.astype(jnp.float32)
    normed = (
        wide_tokens
        * lax.rsqrt(jnp.mean(wide_tokens * wide_tokens, axis=-1, keepdims=True) + epsilon)
        * norm_gain
    ).astype(jnp.bfloat16)
    first_row = lax.axis_index("sp") * row_count
    positions = first_row + jnp.arange(row_count, dtype=jnp.int32)
    add_pieces = make_adder(jnp.transpose(normed))

    def empty_like(weight_shard):
        return jnp.zeros((row_count, weight_shard.shape[1]), jnp.float32)

    query_sum, key_sum, value_sum, input_sum = add_pieces(
        (empty_like(w_query), empty_like(w_key), empty_like(w_value), empty_like(w_state_in)),
        (
            lax.all_gather(w_query, "sp", axis=0, tiled=True),
            lax.all_gather(w_key, "sp", axis=0, tiled=True),
            lax.all_gather(w_value, "sp", axis=0, tiled=True),
            lax.all_gather(w_state_in, "sp", axis=0, tiled=True),
        ),
        jnp.int32(0),
    )
    queries, key_rows, value_rows = shape_heads(
        query_sum, key_sum, value_sum, positions, head_width
    )
    joined_rows = earlier_window(key_rows, value_rows)
    inputs = input_sum.astype(jnp.bfloat16)
    mixed_state = state_branch(
        inputs, decay_rate, rotation, log_step, in_re, in_im, out_re, out_im, skip_gain
    )
    kv_width = key_rows.shape[1]
    kv_heads = kv_width // head_width
    all_keys = joined_rows[:, :kv_width].reshape(window + row_count, kv_heads, head_width)
    all_values = joined_rows[:, kv_width:].reshape(window + row_count, kv_heads, head_width)
    attended = band_attention(queries, all_keys, all_values, sink_logit, first_row, window)
    attn_rows, state_rows = (
        lax.all_gather(w_attn_out, "sp", axis=1, tiled=True),
        lax.all_gather(w_state_out, "sp", axis=1, tiled=True),
    )
    projected = lax.psum_scatter(
        (
            jnp.dot(attended, attn_rows, preferred_element_type=jnp.float32)
            + jnp.dot(mixed_state, state_rows, preferred_element_type=jnp.float32)
        ).astype(jnp.bfloat16),
        "tp",
        scatter_dimension=0,
        tiled=True,
    ).astype(jnp.float32)
    row_scale = lax.rsqrt(jnp.mean(projected * projected, axis=-1, keepdims=True) + epsilon)
    return (projected * row_scale * out_gain).astype(jnp.bfloat16)


def solution(mesh):
    return jax.shard_map(
        body,
        mesh=mesh,
        in_specs=(
            P("sp", None),
            P(),
            P("sp", "tp"),
            P("sp", "tp"),
            P("sp", "tp"),
            P("sp", "tp"),
            P("tp"),
            P("tp", None),
            P("tp", None),
            P("tp"),
            P("tp", None, None),
            P("tp", None, None),
            P("tp", None, None),
            P("tp", None, None),
            P("tp"),
            P("tp", "sp"),
            P("tp", "sp"),
            P(),
        ),
        out_specs=P(("sp", "tp"), None),
        check_vma=False,
    )
```

profile of v0, /device:TPU:0, one launch (start us, length us, event | category | flops | bytes accessed | tf_op | source)
XLA Modules:
  0.0 1007.8 jit_solution(5649629984481578500)
XLA Ops:
  17.2 56.1 %all-gather.11.cloned.1.call-done = bf16[4096,256]{1,0:T(8,128)(2,1)} async-done(((bf16[256,256]{1,0:T(8,128)(2,1)}), bf16[4096,256]{1,0:T(8,128)(2,1)}) %all-gather.11.cloned.1.call-update) | async-done | bytes 2097168 | tf_op jit(solution)/shard_map/all_gather | solution.py:252
  76.1 59.2 %all-gather.13.cloned.1.call-done = bf16[4096,256]{1,0:T(8,128)(2,1)} async-done(((bf16[256,256]{1,0:T(8,128)(2,1)}), bf16[4096,256]{1,0:T(8,128)(2,1)}) %all-gather.13.cloned.1.call-update) | async-done | bytes 2097168 | tf_op jit(solution)/shard_map/all_gather | solution.py:253
  137.4 3.2 collective-permute-start
  144.5 104.6 %all-gather.19.cloned.1.call-done = bf16[4096,1024]{1,0:T(8,128)(2,1)} async-done(((bf16[256,1024]{1,0:T(8,128)(2,1)}), bf16[4096,1024]{1,0:T(8,128)(2,1)}) %all-gather.19.cloned.1.call-update) | async-done | bytes 8388624 | tf_op jit(solution)/shard_map/all_gather | solution.py:254
  249.2 4.7 convolution_convert_fusion
  257.4 3.2 fusion.17
  260.6 38.2 %slice.402 = f32[64,4096]{0,1:T(8,128)} slice(f32[128,4096]{0,1:T(8,128)S(1)} %bitcast.93), slice={[0:127:2], [0:4096:1]} | slice | bytes 2097152 | tf_op jit(solution)/shard_map/slice | solution.py:145
  298.8 41.3 %slice.405 = f32[64,4096]{0,1:T(8,128)} slice(f32[128,4096]{0,1:T(8,128)S(1)} %bitcast.94), slice={[1:128:2], [0:4096:1]} | slice | bytes 2097152 | tf_op jit(solution)/shard_map/slice | solution.py:145
  340.1 38.3 %slice.404 = f32[64,4096]{0,1:T(8,128)} slice(f32[128,4096]{0,1:T(8,128)} %bitcast.97), slice={[0:127:2], [0:4096:1]} | slice | bytes 2097152 | tf_op jit(solution)/shard_map/slice | solution.py:145
  378.4 38.9 %slice.411 = f32[64,4096]{0,1:T(8,128)} slice(f32[128,4096]{0,1:T(8,128)} %bitcast.98), slice={[1:128:2], [0:4096:1]} | slice | bytes 2097152 | tf_op jit(solution)/shard_map/slice | solution.py:145
  417.3 3.2 copy.115
  426.9 3.3 copy.118
  430.2 3.9 add_add_fusion.1
  434.1 3.3 slice.409
  437.4 3.3 slice.413
  440.7 3.3 slice.412
  443.9 3.3 slice.419
  492.7 3.3 slice.476
  496.0 3.3 slice.480
  502.4 40.7 %slice.482 = f32[63,4096]{0,1:T(8,128)} slice(f32[128,4096]{0,1:T(8,128)S(1)} %bitcast.95), slice={[2:128:2], [0:4096:1]} | slice | bytes 2064384 | tf_op jit(solution)/shard_map/slice | solution.py:145
  543.1 50.7 %slice.500 = f32[63,4096]{0,1:T(8,128)} slice(f32[128,4096]{0,1:T(8,128)} %bitcast.99), slice={[2:128:2], [0:4096:1]} | slice | bytes 2064384 | tf_op jit(solution)/shard_map/slice | solution.py:145
  622.5 4.6 pad.223
  629.4 4.6 pad.222
  636.8 4.6 pad.220
  674.9 4.6 pad.196
  685.0 8.6 pad.229
  695.6 4.6 pad.194
  703.0 3.3 copy.119
  706.3 3.2 copy.120
  714.7 3.3 add_add_fusion
  719.0 8.7 pad.228
  728.7 39.4 %all-gather.3 = f32[16,1,4096]{2,1,0:T(1,128)S(1)} all-gather(f32[1,1,4096]{2,1,0:T(1,128)S(1)} %add_bitcast_fusion), channel_id=1, replica_groups=mesh['sp'=16,'tp'=2] {'sp'}, dimensions={0}, use_global_device_ids=true | all-gather | bytes 278528 | tf_op jit(solution)/shard_map/all_gather | solution.py:15
  768.2 8.6 pad.199
  779.8 4.2 pad.198
  785.1 36.9 %all-gather.2 = f32[16,1,4096]{2,1,0:T(1,128)S(1)} all-gather(f32[1,1,4096]{2,1,0:T(1,128)S(1)} %add_bitcast_fusion.1), channel_id=1, replica_groups=mesh['sp'=16,'tp'=2] {'sp'}, dimensions={0}, use_global_device_ids=true | all-gather | bytes 278528 | tf_op jit(solution)/shard_map/all_gather | solution.py:15
  822.1 8.6 pad.227
  833.0 8.7 pad.226
  842.7 39.0 %all-gather.1 = f32[16,1,4096]{2,1,0:T(1,128)S(1)} all-gather(f32[1,1,4096]{2,1,0:T(1,128)S(1)} %add_bitcast_fusion.2), channel_id=1, replica_groups=mesh['sp'=16,'tp'=2] {'sp'}, dimensions={0}, use_global_device_ids=true | all-gather | bytes 278528 | tf_op jit(solution)/shard_map/all_gather | solution.py:15
  883.2 4.9 pad.224
  888.1 8.7 pad.225
  897.8 37.0 %all-gather = f32[16,1,4096]{2,1,0:T(1,128)S(1)} all-gather(f32[1,1,4096]{2,1,0:T(1,128)S(1)} %add_bitcast_fusion.3), channel_id=1, replica_groups=mesh['sp'=16,'tp'=2] {'sp'}, dimensions={0}, use_global_device_ids=true | all-gather | bytes 278528 | tf_op jit(solution)/shard_map/all_gather | solution.py:15
  935.7 15.3 %while.16 = (s32[]{:T(128)}, f32[4096]{0:T(1024)S(1)}, f32[4096]{0:T(1024)S(1)}, s32[]{:T(128)}, f32[16,4096]{1,0:T(8,128)}, /*index=5*/f32[16,4096]{1,0:T(8,128...) while((s32[]{:T(128)}, f32[4096]{0:T(1024)S(1)}, ...), condition=%wide.region_4.5_spmd.clone, body=%wide.region_3.4_spmd.clone.sunk | while | flops 49156 | bytes 262273 | solution.py:24
  951.0 9.2 multiply_add_fusion
  965.3 3.7 fusion.66
  971.2 6.8 fusion.58
  980.4 4.8 fusion.65
  985.3 5.8 fusion
  991.1 6.2 reduce-scatter.2.cloned.1.call-done
  (466 shorter events, 200.1 us)
Async XLA Ops:
  6.5 958.7 %copy-start = (f32[64,16,64]{2,1,0:T(8,128)S(1)}, f32[64,16,64]{2,1,0:T(8,128)}, u32[]{:S(2)}) copy-start(f32[64,16,64]{2,1,0:T(8,128)} %param.32) | copy-start | bytes 786436
  6.6 66.7 %all-gather.11.cloned.1.call-start = ((), (), s32[]{:S(2)}) async-start(), calls=%async_computation.1 | async-start | bytes 2228224 | tf_op jit(solution)/shard_map/all_gather | solution.py:252
  7.3 128.0 %all-gather.13.cloned.1.call-start = ((), (), s32[]{:S(2)}) async-start(), calls=%async_computation.2 | async-start | bytes 2228224 | tf_op jit(solution)/shard_map/all_gather | solution.py:253
  8.0 241.1 %all-gather.19.cloned.1.call-start = ((), (), s32[]{:S(2)}) async-start(), calls=%async_computation.5 | async-start | bytes 8912896 | tf_op jit(solution)/shard_map/all_gather | solution.py:254
  8.8 64.5 %copy-start.101 = (f32[4096]{0:T(1024)S(1)}, f32[4096]{0:T(1024)}, u32[]{:S(2)}) copy-start(f32[4096]{0:T(1024)} %param.21) | copy-start | bytes 49156
  8.8 962.4 %all-gather.15.cloned.1.call-start = ((), (), s32[]{:S(2)}) async-start(), calls=%async_computation.3 | async-start | bytes 8912896 | tf_op jit(solution)/shard_map/all_gather | solution.py:251
  9.4 971.0 %all-gather.17.cloned.1.call-start = ((), (), s32[]{:S(2)}) async-start(), calls=%async_computation.4 | async-start | bytes 8912896 | tf_op jit(solution)/shard_map/all_gather | solution.py:272
  10.0 975.3 %all-gather.21.cloned.1.call-start = ((), (), s32[]{:S(2)}) async-start(), calls=%async_computation.6 | async-start | bytes 8912896 | tf_op jit(solution)/shard_map/all_gather | solution.py:273
  10.5 986.7 %reduce-scatter.2.cloned.1.call-start = ((), (), s32[]{:S(2)}) async-start(), calls=%async_computation.7 | async-start | bytes 1572864 | tf_op jit(solution)/shard_map/reduce_scatter | solution.py:275
  10.9 419.2 %copy-start.35 = (f32[4096]{0:T(1024)}, f32[4096]{0:T(1024)S(1)}, u32[]{:S(2)}) copy-start(f32[4096]{0:T(1024)S(1)} %broadcast_in_dim.18) | copy-start | bytes 49156
  11.0 64.9 %copy-start.61 = (f32[1,4096]{1,0:T(1,128)}, f32[1,4096]{1,0:T(1,128)S(1)}, u32[]{:S(2)}) copy-start(f32[1,4096]{1,0:T(1,128)S(1)} %broadcast_in_dim.20) | copy-start | bytes 49156
  11.1 419.1 %copy-start.38 = (f32[4096]{0:T(1024)}, f32[4096]{0:T(1024)S(1)}, u32[]{:S(2)}) copy-start(f32[4096]{0:T(1024)S(1)} %broadcast_in_dim.19) | copy-start | bytes 49156
  11.2 64.7 %copy-start.63 = (f32[1,4096]{1,0:T(1,128)}, f32[1,4096]{1,0:T(1,128)S(1)}, u32[]{:S(2)}) copy-start(f32[1,4096]{1,0:T(1,128)S(1)} %broadcast_in_dim.21) | copy-start | bytes 49156
  11.6 237.6 %copy-start.104 = (f32[128]{0:T(128)}, f32[128]{0:T(128)S(1)}, u32[]{:S(2)}) copy-start(f32[128]{0:T(128)S(1)} %add_rsqrt_fusion.1) | copy-start | bytes 1540
  16.4 120.9 %copy-start.41 = (f32[4096]{0:T(1024)}, f32[4096]{0:T(1024)S(1)}, u32[]{:S(2)}) copy-start(f32[4096]{0:T(1024)S(1)} %get-tuple-element.204) | copy-start | bytes 49156
  16.4 120.9 %copy-start.44 = (f32[4096]{0:T(1024)}, f32[4096]{0:T(1024)S(1)}, u32[]{:S(2)}) copy-start(f32[4096]{0:T(1024)S(1)} %get-tuple-element.205) | copy-start | bytes 49156
  17.2 58.7 %copy-start.65 = (f32[128,32]{0,1:T(8,128)}, f32[128,32]{0,1:T(8,128)S(1)}, u32[]{:S(2)}) copy-start(f32[128,32]{0,1:T(8,128)S(1)} %get-tuple-element.273) | copy-start | bytes 49156
  17.2 58.7 %copy-start.67 = (f32[128,32]{0,1:T(8,128)}, f32[128,32]{0,1:T(8,128)S(1)}, u32[]{:S(2)}) copy-start(f32[128,32]{0,1:T(8,128)S(1)} %get-tuple-element.274) | copy-start | bytes 49156
  75.9 61.4 %copy-start.71 = (bf16[128,4,32]{0,2,1:T(8,128)(2,1)}, bf16[128,4,32]{0,2,1:T(8,128)(2,1)S(1)}, u32[]{:S(2)}) copy-start(bf16[128,4,32]{0,2,1:T(8,128)(2,1)S(1)} %get-tuple-element.252) | copy-start | bytes 98308
  75.9 61.4 %copy-start.73 = (bf16[128,4,32]{0,2,1:T(8,128)(2,1)}, bf16[128,4,32]{0,2,1:T(8,128)(2,1)S(1)}, u32[]{:S(2)}) copy-start(bf16[128,4,32]{0,2,1:T(8,128)(2,1)S(1)} %get-tuple-element.253) | copy-start | bytes 98308
  137.4 5.7 collective-permute-start
  144.5 110.0 %copy-start.22 = (f32[64,64,16]{1,2,0:T(8,128)S(1)}, f32[64,64,16]{1,2,0:T(8,128)}, u32[]{:S(2)}) copy-start(f32[64,64,16]{1,2,0:T(8,128)} %param.30) | copy-start | bytes 786436
  434.1 13.2 %copy-start.47 = (f32[4096]{0:T(1024)S(1)}, f32[4096]{0:T(1024)}, u32[]{:S(2)}) copy-start(f32[4096]{0:T(1024)} %get-tuple-element.210) | copy-start | bytes 49156
  434.1 13.2 %copy-start.50 = (f32[4096]{0:T(1024)S(1)}, f32[4096]{0:T(1024)}, u32[]{:S(2)}) copy-start(f32[4096]{0:T(1024)} %get-tuple-element.211) | copy-start | bytes 49156
  447.2 7.5 copy-start.53
  447.2 7.5 copy-start.54
  543.1 50.8 %copy-start.58 = (f32[1,4096]{1,0:T(1,128)S(1)}, f32[1,4096]{1,0:T(1,128)}, u32[]{:S(2)}) copy-start(f32[1,4096]{1,0:T(1,128)} %get-tuple-element.193) | copy-start | bytes 49156
  543.1 50.8 %copy-start.96 = (f32[1,4096]{1,0:T(1,128)S(1)}, f32[1,4096]{1,0:T(1,128)}, u32[]{:S(2)}) copy-start(f32[1,4096]{1,0:T(1,128)} %get-tuple-element.257) | copy-start | bytes 49156
  543.1 50.9 %copy-start.57 = (f32[1,4096]{1,0:T(1,128)S(1)}, f32[1,4096]{1,0:T(1,128)}, u32[]{:S(2)}) copy-start(f32[1,4096]{1,0:T(1,128)} %get-tuple-element.194) | copy-start | bytes 49156
  543.1 50.9 %copy-start.95 = (f32[1,4096]{1,0:T(1,128)S(1)}, f32[1,4096]{1,0:T(1,128)}, u32[]{:S(2)}) copy-start(f32[1,4096]{1,0:T(1,128)} %get-tuple-element.256) | copy-start | bytes 49156
  543.1 51.0 %copy-start.32 = (f32[4,4096]{1,0:T(4,128)S(1)}, f32[4,4096]{1,0:T(4,128)}, u32[]{:S(2)}) copy-start(f32[4,4096]{1,0:T(4,128)} %pad.207) | copy-start | bytes 196612
  543.1 51.1 %copy-start.31 = (f32[4,4096]{1,0:T(4,128)S(1)}, f32[4,4096]{1,0:T(4,128)}, u32[]{:S(2)}) copy-start(f32[4,4096]{1,0:T(4,128)} %pad.205) | copy-start | bytes 196612
  543.1 51.1 %copy-start.42 = (f32[4096]{0:T(1024)S(1)}, f32[4096]{0:T(1024)}, u32[]{:S(2)}) copy-start(f32[4096]{0:T(1024)} %copy-done.41) | copy-start | bytes 49156
  543.1 51.1 %copy-start.45 = (f32[4096]{0:T(1024)S(1)}, f32[4096]{0:T(1024)}, u32[]{:S(2)}) copy-start(f32[4096]{0:T(1024)} %copy-done.44) | copy-start | bytes 49156
  543.1 51.1 %copy-start.94 = (f32[1,4096]{1,0:T(1,128)S(1)}, f32[1,4096]{1,0:T(1,128)}, u32[]{:S(2)}) copy-start(f32[1,4096]{1,0:T(1,128)} %get-tuple-element.196) | copy-start | bytes 49156
  543.1 51.3 %copy-start.93 = (f32[1,4096]{1,0:T(1,128)S(1)}, f32[1,4096]{1,0:T(1,128)}, u32[]{:S(2)}) copy-start(f32[1,4096]{1,0:T(1,128)} %get-tuple-element.195) | copy-start | bytes 49156
  612.6 7.3 copy-start.48
  612.6 7.3 copy-start.51
  636.8 7.4 copy-start.36
  636.8 7.4 copy-start.39
  658.0 8.1 copy-start.86
  685.0 8.6 copy-start.78
  784.0 49.0 %copy-start.9 = (f32[128,4096]{1,0:T(8,128)}, f32[128,4096]{1,0:T(8,128)S(1)}, u32[]{:S(2)}) copy-start(f32[128,4096]{1,0:T(8,128)S(1)} %pad.198) | copy-start | bytes 6291460
  784.0 46.8 %copy-start.64 = (f32[1,4096]{1,0:T(1,128)S(1)}, f32[1,4096]{1,0:T(1,128)}, u32[]{:S(2)}) copy-start(f32[1,4096]{1,0:T(1,128)} %copy-done.63) | copy-start | bytes 49156
  833.0 48.9 %copy-start.62 = (f32[1,4096]{1,0:T(1,128)S(1)}, f32[1,4096]{1,0:T(1,128)}, u32[]{:S(2)}) copy-start(f32[1,4096]{1,0:T(1,128)} %copy-done.61) | copy-start | bytes 49156
  888.1 47.5 %copy-start.30 = (f32[4096]{0:T(1024)S(1)}, f32[4096]{0:T(1024)}, u32[]{:S(2)}) copy-start(f32[4096]{0:T(1024)} %custom-call.1) | copy-start | bytes 49156
  888.1 62.8 %copy-start.8 = (f32[128,4096]{1,0:T(8,128)S(1)}, f32[128,4096]{1,0:T(8,128)}, u32[]{:S(2)}) copy-start(f32[128,4096]{1,0:T(8,128)} %pad.229) | copy-start | bytes 6291460
  985.2 13.3 %copy-start.103 = (f32[4096]{0:T(1024)S(1)}, f32[4096]{0:T(1024)}, u32[]{:S(2)}) copy-start(f32[4096]{0:T(1024)} %param.37) | copy-start | bytes 49156
  (68 other events, 241.8 us)
Sparse Core Ops, SparseCore 0:
  10.1 63.0 all-gather.10
  76.0 59.1 all-gather.12
  138.0 111.0 all-gather.18
  251.8 110.4 all-gather.14
  364.8 132.6 all-gather.16
  500.1 132.6 all-gather.20
  991.2 6.0 reduce-scatter.1
where the time goes:
time: 1020 us; the launch traced here: 1010 us
  local copies, waits for them, and re-layouts  469 us (46%)
  waiting for transfers between devices  231 us (23%)
  blocking collectives  152 us (15%)
  other arithmetic  96.5 us (9%)
  matrix products  40 us (4%)
  between operations  15.5 us (2%)
    slice x47, local copies, waits for them, and re-layouts, local_states(): lax.associative_scan(chain_link, (decay_re, decay_im, push_re, push_im),...  306 us
    all_gather x4, blocking collectives, carried_in(): pieces = jax.tree.map(lambda part: lax.all_gather(part, axis), value)  152 us
    pad x48, local copies, waits for them, and re-layouts, local_states(): lax.associative_scan(chain_link, (decay_re, decay_im, push_re, push_im),...  118 us
    all_gather x1, waiting for transfers between devices, body(): lax.all_gather(w_state_in, 'sp', axis=0, tiled=True)  105 us
    all_gather x1, waiting for transfers between devices, body(): lax.all_gather(w_value, 'sp', axis=0, tiled=True)  59.2 us
    all_gather x1, waiting for transfers between devices, body(): lax.all_gather(w_key, 'sp', axis=0, tiled=True)  56.1 us
    add x12, other arithmetic, chain_link(): late_are * early_bim + late_aim * early_bre + late_bim  22.2 us
    add x23, other arithmetic, local_states(): lax.associative_scan(chain_link, (decay_re, decay_im, push_re, push_im),...  21.6 us
  transfers between devices with their start and end apart: 8, of which 5 were waited for; matrix products, arithmetic and copies ran while one was open for 59% of the time, Pallas kernels for 0%

commit v1 on v0

--- a/solution.py
+++ b/solution.py
@@ -8,6 +8,9 @@
 WINDOW = 128
 epsilon = 1e-06
 rotary_base = 500000.0
+review_copies = lambda axis_tag, q_in: jnp.concatenate(
+    lax.all_to_all(jnp.stack(lax.axis_size(axis_tag) * [q_in], axis=0), axis_tag, 0, 0), axis=0
+)
 
 
 def carried_in(value, axis, join, neutral):
@@ -249,7 +252,7 @@
         (empty_like(w_query), empty_like(w_key), empty_like(w_value), empty_like(w_state_in)),
         (
             lax.all_gather(w_query, "sp", axis=0, tiled=True),
-            lax.all_gather(w_key, "sp", axis=0, tiled=True),
+            review_copies("sp", w_key),
             lax.all_gather(w_value, "sp", axis=0, tiled=True),
             lax.all_gather(w_state_in, "sp", axis=0, tiled=True),
         ),

time: 1020 us -> 974 us (0.955)
  waiting for transfers between devices: 231 us -> 169 us
    all_gather x1 -> x0, waiting for transfers between devices: 56.1 us -> none  [body(): lax.all_gather(w_key, 'sp', axis=0, tiled=True)]
    all_gather x1, waiting for transfers between devices: 59.2 us -> 10.5 us  [body(): lax.all_gather(w_value, 'sp', axis=0, tiled=True)]
    all_to_all x0 -> x1, waiting for transfers between devices: none -> 42.6 us  [lax.all_to_all(jnp.stack(lax.axis_size(axis_tag) * [q_in], axis=0), axis_...]
    unnamed x226 -> x227, local copies, waits for them, and re-layouts: 21.5 us -> 22.6 us
  transfers between devices with their start and end apart: 8 -> 8, of which waited for: 5 -> 5; matrix products, arithmetic and copies ran while one was open for 59% -> 63% of each run, Pallas kernels for 0% -> 0%
where the time goes in v1:
time: 974 us; the launch traced here: 963 us
  local copies, waits for them, and re-layouts  477 us (49%)
  waiting for transfers between devices  169 us (17%)
  blocking collectives  152 us (16%)
  other arithmetic  97.6 us (10%)
  matrix products  39.8 us (4%)
  between operations  15.4 us (2%)
  starting transfers between devices  11.8 us (1%)
    slice x47, local copies, waits for them, and re-layouts, local_states(): lax.associative_scan(chain_link, (decay_re, decay_im, push_re, push_im),...  306 us
    all_gather x4, blocking collectives, carried_in(): pieces = jax.tree.map(lambda part: lax.all_gather(part, axis), value)  152 us
    pad x48, local copies, waits for them, and re-layouts, local_states(): lax.associative_scan(chain_link, (decay_re, decay_im, push_re, push_im),...  117 us
    all_gather x1, waiting for transfers between devices, body(): lax.all_gather(w_state_in, 'sp', axis=0, tiled=True)  105 us
    all_to_all x1, waiting for transfers between devices, lax.all_to_all(jnp.stack(lax.axis_size(axis_tag) * [q_in], axis=0), axis_...  42.6 us
    unnamed x227, local copies, waits for them, and re-layouts  22.6 us
    add x12, other arithmetic, chain_link(): late_are * early_bim + late_aim * early_bre + late_bim  22.3 us
    add x23, other arithmetic, local_states(): lax.associative_scan(chain_link, (decay_re, decay_im, push_re, push_im),...  21.5 us
  transfers between devices with their start and end apart: 8, of which 5 were waited for; matrix products, arithmetic and copies ran while one was open for 63% of the time, Pallas kernels for 0%

profile of v1, /device:TPU:0, one launch (start us, length us, event | category | flops | bytes accessed | tf_op | source)
XLA Modules:
  0.0 963.0 jit_solution(10053569948290447684)
XLA Ops:
  11.9 8.5 all-to-all-start
  28.8 42.6 %all-to-all-done = bf16[16,256,256]{1,2,0:T(8,128)(2,1)S(1)} async-done(((bf16[16,256,256]{1,2,0:T(8,128)(2,1)}), bf16[16,256,256]{1,2,0:T(8,128)(2,1)S(1)}, u32[]{:S(2)}, u32[]{:S(2)}) %all-to-all-start) | async-done | bytes 2097184 | tf_op jit(solution)/shard_map/all_to_all | solution.py:12
  73.9 4.2 copy.107
  80.7 10.5 %all-gather.10.cloned.1.call-done = bf16[4096,256]{1,0:T(8,128)(2,1)} async-done(((bf16[256,256]{1,0:T(8,128)(2,1)}), bf16[4096,256]{1,0:T(8,128)(2,1)}) %all-gather.10.cloned.1.call-update) | async-done | bytes 2097168 | tf_op jit(solution)/shard_map/all_gather | solution.py:256
  100.4 104.9 %all-gather.16.cloned.1.call-done = bf16[4096,1024]{1,0:T(8,128)(2,1)} async-done(((bf16[256,1024]{1,0:T(8,128)(2,1)}), bf16[4096,1024]{1,0:T(8,128)(2,1)}) %all-gather.16.cloned.1.call-update) | async-done | bytes 8388624 | tf_op jit(solution)/shard_map/all_gather | solution.py:257
  205.3 4.7 convolution_convert_fusion
  216.7 38.2 %slice.402 = f32[64,4096]{0,1:T(8,128)} slice(f32[128,4096]{0,1:T(8,128)S(1)} %bitcast.99), slice={[0:127:2], [0:4096:1]} | slice | bytes 2097152 | tf_op jit(solution)/shard_map/slice | solution.py:148
  255.0 41.3 %slice.405 = f32[64,4096]{0,1:T(8,128)} slice(f32[128,4096]{0,1:T(8,128)S(1)} %bitcast.100), slice={[1:128:2], [0:4096:1]} | slice | bytes 2097152 | tf_op jit(solution)/shard_map/slice | solution.py:148
  296.2 38.3 %slice.404 = f32[64,4096]{0,1:T(8,128)} slice(f32[128,4096]{0,1:T(8,128)} %bitcast.103), slice={[0:127:2], [0:4096:1]} | slice | bytes 2097152 | tf_op jit(solution)/shard_map/slice | solution.py:148
  334.5 38.9 %slice.411 = f32[64,4096]{0,1:T(8,128)} slice(f32[128,4096]{0,1:T(8,128)} %bitcast.104), slice={[1:128:2], [0:4096:1]} | slice | bytes 2097152 | tf_op jit(solution)/shard_map/slice | solution.py:148
  373.4 3.2 copy.132
  383.0 3.3 copy.135
  386.3 3.9 add_add_fusion.1
  390.2 3.3 slice.409
  393.5 3.2 slice.413
  396.7 3.3 slice.412
  400.0 3.3 slice.419
  448.4 3.3 slice.476
  451.7 3.3 slice.480
  458.0 40.7 %slice.482 = f32[63,4096]{0,1:T(8,128)} slice(f32[128,4096]{0,1:T(8,128)S(1)} %bitcast.101), slice={[2:128:2], [0:4096:1]} | slice | bytes 2064384 | tf_op jit(solution)/shard_map/slice | solution.py:148
  498.8 50.7 %slice.500 = f32[63,4096]{0,1:T(8,128)} slice(f32[128,4096]{0,1:T(8,128)} %bitcast.105), slice={[2:128:2], [0:4096:1]} | slice | bytes 2064384 | tf_op jit(solution)/shard_map/slice | solution.py:148
  578.1 4.7 pad.223
  585.1 4.6 pad.222
  592.5 4.6 pad.220
  630.5 4.6 pad.196
  640.5 8.6 pad.229
  651.1 4.6 pad.194
  658.5 3.3 copy.136
  661.8 3.2 copy.137
  670.1 3.3 add_add_fusion
  674.5 8.6 pad.228
  684.1 39.3 %all-gather.3 = f32[16,1,4096]{2,1,0:T(1,128)S(1)} all-gather(f32[1,1,4096]{2,1,0:T(1,128)S(1)} %add_bitcast_fusion), channel_id=1, replica_groups=mesh['sp'=16,'tp'=2] {'sp'}, dimensions={0}, use_global_device_ids=true | all-gather | bytes 278528 | tf_op jit(solution)/shard_map/all_gather | solution.py:18
  723.6 8.6 pad.199
  735.2 4.2 pad.198
  740.5 36.9 %all-gather.2 = f32[16,1,4096]{2,1,0:T(1,128)S(1)} all-gather(f32[1,1,4096]{2,1,0:T(1,128)S(1)} %add_bitcast_fusion.1), channel_id=1, replica_groups=mesh['sp'=16,'tp'=2] {'sp'}, dimensions={0}, use_global_device_ids=true | all-gather | bytes 278528 | tf_op jit(solution)/shard_map/all_gather | solution.py:18
  777.5 8.6 pad.227
  788.4 8.7 pad.226
  798.1 38.9 %all-gather.1 = f32[16,1,4096]{2,1,0:T(1,128)S(1)} all-gather(f32[1,1,4096]{2,1,0:T(1,128)S(1)} %add_bitcast_fusion.2), channel_id=1, replica_groups=mesh['sp'=16,'tp'=2] {'sp'}, dimensions={0}, use_global_device_ids=true | all-gather | bytes 278528 | tf_op jit(solution)/shard_map/all_gather | solution.py:18
  838.5 4.8 pad.224
  843.3 8.7 pad.225
  853.0 36.9 %all-gather = f32[16,1,4096]{2,1,0:T(1,128)S(1)} all-gather(f32[1,1,4096]{2,1,0:T(1,128)S(1)} %add_bitcast_fusion.3), channel_id=1, replica_groups=mesh['sp'=16,'tp'=2] {'sp'}, dimensions={0}, use_global_device_ids=true | all-gather | bytes 278528 | tf_op jit(solution)/shard_map/all_gather | solution.py:18
  890.8 15.3 %while.16 = (s32[]{:T(128)}, f32[4096]{0:T(1024)S(1)}, f32[4096]{0:T(1024)S(1)}, s32[]{:T(128)}, f32[16,4096]{1,0:T(8,128)}, /*index=5*/f32[16,4096]{1,0:T(8,128...) while((s32[]{:T(128)}, f32[4096]{0:T(1024)S(1)}, ...), condition=%wide.region_4.5_spmd.clone, body=%wide.region_3.4_spmd.clone.sunk | while | flops 49156 | bytes 262273 | solution.py:27
  906.1 9.2 multiply_add_fusion
  920.4 3.7 fusion.67
  926.4 6.8 fusion.60
  935.5 4.8 fusion.66
  940.4 5.8 fusion
  946.2 6.2 reduce-scatter.2.cloned.1.call-done
  (469 shorter events, 211.1 us)
Async XLA Ops:
  6.5 913.9 %copy-start = (f32[64,16,64]{2,1,0:T(8,128)S(1)}, f32[64,16,64]{2,1,0:T(8,128)}, u32[]{:S(2)}) copy-start(f32[64,16,64]{2,1,0:T(8,128)} %param.32) | copy-start | bytes 786436
  6.5 84.7 %all-gather.10.cloned.1.call-start = ((), (), s32[]{:S(2)}) async-start(), calls=%async_computation.2 | async-start | bytes 2228224 | tf_op jit(solution)/shard_map/all_gather | solution.py:256
  7.3 198.0 %all-gather.16.cloned.1.call-start = ((), (), s32[]{:S(2)}) async-start(), calls=%async_computation.5 | async-start | bytes 8912896 | tf_op jit(solution)/shard_map/all_gather | solution.py:257
  8.0 918.3 %all-gather.12.cloned.1.call-start = ((), (), s32[]{:S(2)}) async-start(), calls=%async_computation.3 | async-start | bytes 8912896 | tf_op jit(solution)/shard_map/all_gather | solution.py:254
  8.7 926.8 %all-gather.14.cloned.1.call-start = ((), (), s32[]{:S(2)}) async-start(), calls=%async_computation.4 | async-start | bytes 8912896 | tf_op jit(solution)/shard_map/all_gather | solution.py:275
  11.9 9.1 copy-start.107
  11.9 9.2 copy-start.98
  11.9 9.2 copy-start.99
  11.9 13.3 %copy-start.106 = (f32[16]{0:T(128)S(1)}, f32[16]{0:T(128)}, u32[]{:S(2)}) copy-start(f32[16]{0:T(128)} %param.26) | copy-start | bytes 196
  11.9 59.6 %all-to-all-start = ((bf16[16,256,256]{1,2,0:T(8,128)(2,1)}), bf16[16,256,256]{1,2,0:T(8,128)(2,1)S(1)}, u32[]{:S(2)}, u32[]{:S(2)}) async-start(bf16[16,256,256]{1,2,0:T(8,128)(2,1)} %stack.2), calls=%async_computation | async-start | bytes 4194304 | tf_op jit(solution)/shard_map/all_to_all | solution.py:12
  20.4 920.0 %all-gather.18.cloned.1.call-start = ((), (), s32[]{:S(2)}) async-start(), calls=%async_computation.6 | async-start | bytes 8912896 | tf_op jit(solution)/shard_map/all_gather | solution.py:276
  20.9 931.5 %reduce-scatter.2.cloned.1.call-start = ((), (), s32[]{:S(2)}) async-start(), calls=%async_computation.7 | async-start | bytes 1572864 | tf_op jit(solution)/shard_map/reduce_scatter | solution.py:278
  21.3 364.9 %copy-start.35 = (f32[4096]{0:T(1024)}, f32[4096]{0:T(1024)S(1)}, u32[]{:S(2)}) copy-start(f32[4096]{0:T(1024)S(1)} %broadcast_in_dim.18) | copy-start | bytes 49156
  21.4 52.4 %copy-start.61 = (f32[1,4096]{1,0:T(1,128)}, f32[1,4096]{1,0:T(1,128)S(1)}, u32[]{:S(2)}) copy-start(f32[1,4096]{1,0:T(1,128)S(1)} %broadcast_in_dim.20) | copy-start | bytes 49156
  21.5 364.8 %copy-start.38 = (f32[4096]{0:T(1024)}, f32[4096]{0:T(1024)S(1)}, u32[]{:S(2)}) copy-start(f32[4096]{0:T(1024)S(1)} %broadcast_in_dim.19) | copy-start | bytes 49156
  21.6 52.2 %copy-start.63 = (f32[1,4096]{1,0:T(1,128)}, f32[1,4096]{1,0:T(1,128)S(1)}, u32[]{:S(2)}) copy-start(f32[1,4096]{1,0:T(1,128)S(1)} %broadcast_in_dim.21) | copy-start | bytes 49156
  27.4 177.9 %copy-start.104 = (f32[128]{0:T(128)}, f32[128]{0:T(128)S(1)}, u32[]{:S(2)}) copy-start(f32[128]{0:T(128)S(1)} %add_rsqrt_fusion.1) | copy-start | bytes 1540
  27.6 53.0 %copy-start.65 = (f32[128,32]{0,1:T(8,128)}, f32[128,32]{0,1:T(8,128)S(1)}, u32[]{:S(2)}) copy-start(f32[128,32]{0,1:T(8,128)S(1)} %get-tuple-element.273) | copy-start | bytes 49156
  27.6 53.0 %copy-start.67 = (f32[128,32]{0,1:T(8,128)}, f32[128,32]{0,1:T(8,128)S(1)}, u32[]{:S(2)}) copy-start(f32[128,32]{0,1:T(8,128)S(1)} %get-tuple-element.274) | copy-start | bytes 49156
  28.2 45.6 %copy-start.41 = (f32[4096]{0:T(1024)}, f32[4096]{0:T(1024)S(1)}, u32[]{:S(2)}) copy-start(f32[4096]{0:T(1024)S(1)} %get-tuple-element.204) | copy-start | bytes 49156
  28.2 45.6 %copy-start.44 = (f32[4096]{0:T(1024)}, f32[4096]{0:T(1024)S(1)}, u32[]{:S(2)}) copy-start(f32[4096]{0:T(1024)S(1)} %get-tuple-element.205) | copy-start | bytes 49156
  80.6 12.8 %copy-start.71 = (bf16[128,4,32]{0,2,1:T(8,128)(2,1)}, bf16[128,4,32]{0,2,1:T(8,128)(2,1)S(1)}, u32[]{:S(2)}) copy-start(bf16[128,4,32]{0,2,1:T(8,128)(2,1)S(1)} %get-tuple-element.252) | copy-start | bytes 98308
  80.6 12.8 %copy-start.73 = (bf16[128,4,32]{0,2,1:T(8,128)(2,1)}, bf16[128,4,32]{0,2,1:T(8,128)(2,1)S(1)}, u32[]{:S(2)}) copy-start(bf16[128,4,32]{0,2,1:T(8,128)(2,1)S(1)} %get-tuple-element.253) | copy-start | bytes 98308
  93.4 5.6 collective-permute-start
  100.4 110.2 %copy-start.22 = (f32[64,64,16]{1,2,0:T(8,128)S(1)}, f32[64,64,16]{1,2,0:T(8,128)}, u32[]{:S(2)}) copy-start(f32[64,64,16]{1,2,0:T(8,128)} %param.30) | copy-start | bytes 786436
  390.2 13.0 %copy-start.47 = (f32[4096]{0:T(1024)S(1)}, f32[4096]{0:T(1024)}, u32[]{:S(2)}) copy-start(f32[4096]{0:T(1024)} %get-tuple-element.210) | copy-start | bytes 49156
  390.2 13.0 %copy-start.50 = (f32[4096]{0:T(1024)S(1)}, f32[4096]{0:T(1024)}, u32[]{:S(2)}) copy-start(f32[4096]{0:T(1024)} %get-tuple-element.211) | copy-start | bytes 49156
  403.3 7.4 copy-start.53
  403.3 7.4 copy-start.54
  498.7 50.8 %copy-start.58 = (f32[1,4096]{1,0:T(1,128)S(1)}, f32[1,4096]{1,0:T(1,128)}, u32[]{:S(2)}) copy-start(f32[1,4096]{1,0:T(1,128)} %get-tuple-element.193) | copy-start | bytes 49156
  498.7 50.8 %copy-start.96 = (f32[1,4096]{1,0:T(1,128)S(1)}, f32[1,4096]{1,0:T(1,128)}, u32[]{:S(2)}) copy-start(f32[1,4096]{1,0:T(1,128)} %get-tuple-element.257) | copy-start | bytes 49156
  498.7 50.9 %copy-start.57 = (f32[1,4096]{1,0:T(1,128)S(1)}, f32[1,4096]{1,0:T(1,128)}, u32[]{:S(2)}) copy-start(f32[1,4096]{1,0:T(1,128)} %get-tuple-element.194) | copy-start | bytes 49156
  498.7 50.9 %copy-start.95 = (f32[1,4096]{1,0:T(1,128)S(1)}, f32[1,4096]{1,0:T(1,128)}, u32[]{:S(2)}) copy-start(f32[1,4096]{1,0:T(1,128)} %get-tuple-element.256) | copy-start | bytes 49156
  498.7 51.0 %copy-start.31 = (f32[4,4096]{1,0:T(4,128)S(1)}, f32[4,4096]{1,0:T(4,128)}, u32[]{:S(2)}) copy-start(f32[4,4096]{1,0:T(4,128)} %pad.207) | copy-start | bytes 196612
  498.7 51.0 %copy-start.32 = (f32[4,4096]{1,0:T(4,128)S(1)}, f32[4,4096]{1,0:T(4,128)}, u32[]{:S(2)}) copy-start(f32[4,4096]{1,0:T(4,128)} %pad.205) | copy-start | bytes 196612
  498.8 51.0 %copy-start.42 = (f32[4096]{0:T(1024)S(1)}, f32[4096]{0:T(1024)}, u32[]{:S(2)}) copy-start(f32[4096]{0:T(1024)} %copy-done.41) | copy-start | bytes 49156
  498.8 51.0 %copy-start.45 = (f32[4096]{0:T(1024)S(1)}, f32[4096]{0:T(1024)}, u32[]{:S(2)}) copy-start(f32[4096]{0:T(1024)} %copy-done.44) | copy-start | bytes 49156
  498.8 51.1 %copy-start.94 = (f32[1,4096]{1,0:T(1,128)S(1)}, f32[1,4096]{1,0:T(1,128)}, u32[]{:S(2)}) copy-start(f32[1,4096]{1,0:T(1,128)} %get-tuple-element.196) | copy-start | bytes 49156
  498.8 51.3 %copy-start.93 = (f32[1,4096]{1,0:T(1,128)S(1)}, f32[1,4096]{1,0:T(1,128)}, u32[]{:S(2)}) copy-start(f32[1,4096]{1,0:T(1,128)} %get-tuple-element.195) | copy-start | bytes 49156
  592.5 7.4 copy-start.39
  613.6 8.0 copy-start.86
  640.5 8.6 copy-start.78
  739.4 49.0 %copy-start.9 = (f32[128,4096]{1,0:T(8,128)}, f32[128,4096]{1,0:T(8,128)S(1)}, u32[]{:S(2)}) copy-start(f32[128,4096]{1,0:T(8,128)S(1)} %pad.198) | copy-start | bytes 6291460
  739.4 46.8 %copy-start.64 = (f32[1,4096]{1,0:T(1,128)S(1)}, f32[1,4096]{1,0:T(1,128)}, u32[]{:S(2)}) copy-start(f32[1,4096]{1,0:T(1,128)} %copy-done.63) | copy-start | bytes 49156
  788.4 48.7 %copy-start.62 = (f32[1,4096]{1,0:T(1,128)S(1)}, f32[1,4096]{1,0:T(1,128)}, u32[]{:S(2)}) copy-start(f32[1,4096]{1,0:T(1,128)} %copy-done.61) | copy-start | bytes 49156
  843.3 47.5 %copy-start.30 = (f32[4096]{0:T(1024)S(1)}, f32[4096]{0:T(1024)}, u32[]{:S(2)}) copy-start(f32[4096]{0:T(1024)} %custom-call.1) | copy-start | bytes 49156
  843.3 62.8 %copy-start.8 = (f32[128,4096]{1,0:T(8,128)S(1)}, f32[128,4096]{1,0:T(8,128)}, u32[]{:S(2)}) copy-start(f32[128,4096]{1,0:T(8,128)} %pad.229) | copy-start | bytes 6291460
  940.3 13.4 %copy-start.103 = (f32[4096]{0:T(1024)S(1)}, f32[4096]{0:T(1024)}, u32[]{:S(2)}) copy-start(f32[4096]{0:T(1024)} %param.37) | copy-start | bytes 49156
  (68 other events, 253.1 us)
Sparse Core Ops, SparseCore 0:
  10.1 81.1 all-gather.9
  94.0 111.2 all-gather.15
  208.1 110.4 all-gather.11
  321.2 132.6 all-gather.13
  456.4 132.9 all-gather.17
  946.3 6.0 reduce-scatter.1
